TPU v7x, 32 devices: a whole 2x2x4 slice. The times are simulated.
32 devices in a mesh: sp: 4 (over z), dp: 8 (over y, x, core).
Axes of the slice: x: 2, y: 2, z: 4, core: 2. Of those that a mesh axis runs over, the one named last changes fastest.
Arguments:
- probe_vectors: bfloat16 [4096, 1024], P(('dp', 'sp')), may hold values from -6 to 6
- address_vectors: bfloat16 [4096, 1024], P(('dp', 'sp')), may hold values from -6 to 6
- content_vectors: bfloat16 [4096, 2048], P(('dp', 'sp')), may hold values from -6 to 6
- adjoint_of_result: bfloat16 [4096, 2048], P(('dp', 'sp')), may hold values from -0.5 to 0.5
- compact_factor: bfloat16 [4096, 64], P(('dp', 'sp')), may hold values from -7.5 to 7.5
- latent_to_damping_map: bfloat16 [64, 1024], replicated, may hold values from -0.75 to 0.75
- damping_shift_term: float32 [1024], replicated
- surplus_damping: bfloat16 [4096, 16], P(('dp', 'sp')), may hold values from -0.7 to 0
Outputs:
- query_grad: bfloat16 [4096, 1024], P(('dp', 'sp'))
- key_grad: bfloat16 [4096, 1024], P(('dp', 'sp'))
- value_grad: bfloat16 [4096, 2048], P(('dp', 'sp'))
- latent_grad: bfloat16 [4096, 64], P(('dp', 'sp'))
- weight_grad: float32 [64, 1024], replicated
All inputs are finite; a program needn't handle non-finite values.
Results may differ from a plain program's by a relative error of at most 0.005.
Values may be sent and summed in bfloat16 or wider, within the bound.
No kernel may reach another device: no remote copies, remote signals or barrier semaphores. Data moves between devices by JAX's collectives and lax.ppermute only.
A program may use at most 64 MiB of HBM per device.

v0:
```python
import jax
import jax.numpy as jnp
from jax import lax
from jax.sharding import PartitionSpec as P

KEY_CHANNELS = 64
VALUE_DIM = 128
BLOCK = 64


gate_norm = 16.0
highest = lax.Precision.HIGHEST


def carry_states(block_total, increments):
    log_totals = block_total[:, :, 0, :]
    running = jnp.cumsum(log_totals, axis=1)
    before = running - log_totals
    blocks = log_totals.shape[1]
    order = jnp.arange(blocks, dtype=jnp.int32)
    earlier_mask = (order[None, :] < order[:, None])[None, :, :, None]
    exponent = before[:, :, None, :] - running[:, None, :, :]
    exponent = jnp.where(earlier_mask, exponent, jnp.zeros_like(exponent))
    weights = jnp.where(earlier_mask, jnp.exp(exponent), jnp.zeros_like(exponent))
    return jnp.einsum("hnmk,mhkv->nhkv", weights, increments, precision=highest)


def gla_forward(probe_vectors, address_vectors, content_vectors, logarithm_decay):
    head_count, seq_len, key_width = probe_vectors.shape
    value_width = content_vectors.shape[2]
    blocks = seq_len // BLOCK

    def blocked(tensor):
        return tensor.reshape(head_count, blocks, BLOCK, tensor.shape[2])

    cumulative = jnp.cumsum(blocked(logarithm_decay), axis=2)
    block_total = cumulative[:, :, BLOCK - 1 :, :]
    keys_block = blocked(address_vectors)
    query_decayed = blocked(probe_vectors) * key_width ** (-0.5) * jnp.exp(cumulative)
    key_inverse = keys_block * jnp.exp(-cumulative)
    key_to_end = keys_block * jnp.exp(block_total - cumulative)
    value_block = blocked(content_vectors)
    scores = jnp.einsum("hnik,hnjk->hnij", query_decayed, key_inverse, precision=highest)
    positions = jnp.arange(BLOCK, dtype=jnp.int32)
    causal = positions[:, None] >= positions[None, :]
    scores = jnp.where(causal, scores, jnp.zeros_like(scores))
    within_block = jnp.einsum("hnij,hnjv->hniv", scores, value_block, precision=highest)
    increments = jnp.einsum("hnjk,hnjv->nhkv", key_to_end, value_block, precision=highest)
    earlier = carry_states(block_total, increments)
    carried = jnp.einsum("hnik,nhkv->hniv", query_decayed, earlier, precision=highest)
    return (within_block + carried).reshape(head_count, seq_len, value_width)


def split_into_heads(tensor, width):
    return tensor.astype(jnp.float32).reshape(tensor.shape[0], -1, width).transpose(1, 0, 2)


def to_rows(tensor):
    return tensor.transpose(1, 0, 2).reshape(tensor.shape[1], tensor.shape[0] * tensor.shape[2])


def on_device(
    probe_vectors,
    address_vectors,
    content_vectors,
    adjoint_of_result,
    compact_factor,
    latent_to_damping_map,
    damping_shift_term,
    surplus_damping,
):
    query_per_head, key_per_head, value_per_head, upstream_heads, spike_heads = (
        lax.all_to_all(probe_vectors, "sp", split_axis=1, concat_axis=0, tiled=True),
        lax.all_to_all(address_vectors, "sp", split_axis=1, concat_axis=0, tiled=True),
        lax.all_to_all(content_vectors, "sp", split_axis=1, concat_axis=0, tiled=True),
        lax.all_to_all(adjoint_of_result, "sp", split_axis=1, concat_axis=0, tiled=True),
        lax.all_to_all(surplus_damping, "sp", split_axis=1, concat_axis=0, tiled=True),
    )
    local_width = query_per_head.shape[1]
    hidden_code_rows = lax.all_gather(compact_factor, "sp", axis=0, tiled=True)
    column_start = lax.axis_index("sp") * local_width
    weight_local = lax.dynamic_slice_in_dim(latent_to_damping_map, column_start, local_width, 1)
    bias_local = lax.dynamic_slice_in_dim(damping_shift_term, column_start, local_width, 0)
    gate_logit = (
        jnp.dot(hidden_code_rows, weight_local, preferred_element_type=jnp.float32) + bias_local
    )
    forget_rate_rows = jax.nn.log_sigmoid(gate_logit) / gate_norm
    logarithm_decay = (
        split_into_heads(forget_rate_rows, KEY_CHANNELS)
        + spike_heads.astype(jnp.float32).T[:, :, None]
    )
    _, pullback = jax.vjp(
        gla_forward,
        split_into_heads(query_per_head, KEY_CHANNELS),
        split_into_heads(key_per_head, KEY_CHANNELS),
        split_into_heads(value_per_head, VALUE_DIM),
        logarithm_decay,
    )
    grad_query, grad_key, grad_value, grad_decay = pullback(
        split_into_heads(upstream_heads, VALUE_DIM)
    )
    query_grad, key_grad, value_grad = (
        lax.all_to_all(
            to_rows(grad_query).astype(jnp.bfloat16), "sp", split_axis=0, concat_axis=1, tiled=True
        ),
        lax.all_to_all(
            to_rows(grad_key).astype(jnp.bfloat16), "sp", split_axis=0, concat_axis=1, tiled=True
        ),
        lax.all_to_all(
            to_rows(grad_value).astype(jnp.bfloat16), "sp", split_axis=0, concat_axis=1, tiled=True
        ),
    )
    decay_rows = to_rows(grad_decay)
    gate_grad = (decay_rows * jax.nn.sigmoid(-gate_logit) / gate_norm).astype(jnp.bfloat16)
    partial_latent = jnp.einsum(
        "sc,rc->sr", gate_grad, weight_local, preferred_element_type=jnp.float32
    )
    latent_grad = lax.psum_scatter(partial_latent, "sp", scatter_dimension=0, tiled=True).astype(
        jnp.bfloat16
    )
    local_weight = jnp.einsum(
        "sr,sc->rc", hidden_code_rows, gate_grad, preferred_element_type=jnp.float32
    )
    summed = lax.psum(local_weight, "dp")
    weight_grad = lax.all_gather(summed, "sp", axis=1, tiled=True)
    return (query_grad, key_grad, value_grad, latent_grad, weight_grad)


def solution(mesh):
    return jax.shard_map(
        on_device,
        mesh=mesh,
        in_specs=(
            P(("dp", "sp"), None),
            P(("dp", "sp"), None),
            P(("dp", "sp"), None),
            P(("dp", "sp"), None),
            P(("dp", "sp"), None),
            P(),
            P(),
            P(("dp", "sp"), None),
        ),
        out_specs=(
            P(("dp", "sp"), None),
            P(("dp", "sp"), None),
            P(("dp", "sp"), None),
            P(("dp", "sp"), None),
            P(),
        ),
        check_vma=False,
    )
```

profile of v0, /device:TPU:0, one launch (start us, length us, event | category | flops | bytes accessed | tf_op | source)
XLA Modules:
  0.0 277.0 jit_solution(3052615414394250195)
XLA Ops:
  8.0 6.5 %all-to-all-start.1 = ((bf16[128,4,4]{0,2,1:T(4,128)(2,1)}), bf16[128,4,4]{0,2,1:T(4,128)(2,1)S(1)}, u32[]{:S(2)}, u32[]{:S(2)}) async-start(bf16[128,4,4]{0,2,1:T(4,128)(2,1)} %bitcast.169), calls=%async_computation.1 | async-start | bytes 8192 | tf_op jit(solution)/shard_map/all_to_all | solution.py:77
  16.3 3.8 %all-to-all-done.1 = bf16[128,4,4]{0,2,1:T(4,128)(2,1)S(1)} async-done(((bf16[128,4,4]{0,2,1:T(4,128)(2,1)}), bf16[128,4,4]{0,2,1:T(4,128)(2,1)S(1)}, u32[]{:S(2)}, u32[]{:S(2)}) %all-to-all-start.1) | async-done | bytes 4128 | tf_op jit(solution)/shard_map/all_to_all | solution.py:77
  20.1 3.5 %all-to-all-start.5 = ((bf16[128,4,256]{0,2,1:T(8,128)(2,1)}), bf16[128,4,256]{0,2,1:T(8,128)(2,1)S(1)}, u32[]{:S(2)}, u32[]{:S(2)}) async-start(bf16[128,4,256]{0,2,1:T(8,128)(2,1)} %bitcast.24), calls=%async_computation.5 | async-start | bytes 524288 | tf_op jit(solution)/shard_map/all_to_all | solution.py:73
  24.5 7.0 %all-to-all-done.5 = bf16[128,4,256]{0,2,1:T(8,128)(2,1)S(1)} async-done(((bf16[128,4,256]{0,2,1:T(8,128)(2,1)}), bf16[128,4,256]{0,2,1:T(8,128)(2,1)S(1)}, u32[]{:S(2)}, u32[]{:S(2)}) %all-to-all-start.5) | async-done | bytes 262176 | tf_op jit(solution)/shard_map/all_to_all | solution.py:73
  31.5 3.4 %all-to-all-start = ((bf16[128,4,256]{0,2,1:T(8,128)(2,1)}), bf16[128,4,256]{0,2,1:T(8,128)(2,1)S(1)}, u32[]{:S(2)}, u32[]{:S(2)}) async-start(bf16[128,4,256]{0,2,1:T(8,128)(2,1)} %bitcast), calls=%async_computation | async-start | bytes 524288 | tf_op jit(solution)/shard_map/all_to_all | solution.py:74
  36.6 12.5 %all_gather.6 = bf16[512,64]{0,1:T(8,128)(2,1)S(1)} all-gather(bf16[128,64]{0,1:T(8,128)(2,1)S(1)} %copy-done.31), channel_id=1, replica_groups=mesh['sp'=4,'dp'=8] {'sp'}, dimensions={0}, use_global_device_ids=true | all-gather | bytes 81920 | tf_op jit(solution)/shard_map/all_gather | solution.py:80
  51.7 4.1 %all-to-all-start.3 = ((bf16[128,4,512]{2,0,1:T(8,128)(2,1)}), bf16[128,4,512]{2,0,1:T(8,128)(2,1)}, u32[]{:S(2)}, u32[]{:S(2)}) async-start(bf16[128,4,512]{2,0,1:T(8,128)(2,1)} %bitcast.143), calls=%async_computation.3 | async-start | bytes 1048576 | tf_op jit(solution)/shard_map/all_to_all | solution.py:76
  58.0 25.9 %fusion.46 = f32[4,8,64,64]{3,1,2,0:T(8,128)S(1)} fusion(f32[4,8,64,64]{3,1,2,0:T(8,128)S(1)} %copy.194), kind=kOutput, calls=%fused_computation.84 | output fusion | flops 8257536 | bytes 1048576 | tf_op jit(solution)/shard_map/jvp(jit(cumsum))/reduce_window_sum | solution.py:36
  83.9 5.1 %all-to-all-start.2 = ((bf16[128,4,512]{2,0,1:T(8,128)(2,1)}), bf16[128,4,512]{2,0,1:T(8,128)(2,1)}, u32[]{:S(2)}, u32[]{:S(2)}) async-start(bf16[128,4,512]{2,0,1:T(8,128)(2,1)} %bitcast.144), calls=%async_computation.2 | async-start | bytes 1048576 | tf_op jit(solution)/shard_map/all_to_all | solution.py:75
  95.1 2.0 reshape.161
  99.4 2.0 reshape.159
  103.7 2.9 %convolution_bitcast_fusion = f32[8,4,64,128]{3,0,2,1:T(8,128)S(1)} fusion(f32[4,64,128,8]{2,1,3,0:T(8,128)S(1)} %convolution_bitcast_fusion.3, f32[4,8,64]{1,2,0:T(8,128)S(1)} %copy-done.23, f32[4,8,64]{1,2,0:T(8,128)S(1)} %copy-done.24, pred[8,8]{1,0:T(8,128)(4,1)S(1)} %copy-done.32), kind=kOutput, calls=%fused_computation.4 | convolution fusion | flops 25214976 | bytes 2113600 | tf_op jit(solution)/shard_map/transpose(jvp(hnmk,mhkv->nhkv))/dot_general | solution.py:25
  106.6 2.8 %fusion.18 = (f32[4,8,64]{2,1,0:T(8,128)}, f32[4,8,64,64]{2,3,1,0:T(8,128)S(1)}, f32[4,8,64,64]{2,3,1,0:T(8,128)}) fusion(f32[4,8,64,64]{2,3,1,0:T(8,128)S(1)} %copy.195, f32[4,8,64,64]{2,1,3,0:T(8,128)S(1)} %reshape.166, f32[4,8,64]{2,1,0:T(8,128)S(1)} %slice_bitcast_fusion, bf16[4,8,64,128]{3,2,1,0:T(8,128)(2,1)S(1)} %bitcast.150, ...), kind=kOutput, calls=%fused_computation.40 | convolution fusion | flops 201979904 | bytes 3686400 | tf_op jit(solution)/shard_map/transpose(jvp(hnjk,hnjv->nhkv))/dot_general | solution.py:48
  110.4 2.5 convolution_bitcast_fusion.1
  112.9 4.3 %fusion.45 = (f32[4,8,64]{1,2,0:T(8,128)}, f32[4,8,64]{1,2,0:T(8,128)}) fusion(f32[4,8,64]{1,2,0:T(8,128)S(1)} %copy-done.23, f32[4,8,64]{1,2,0:T(8,128)S(1)} %copy-done.24, f32[8,4,64,128]{3,2,1,0:T(8,128)S(1)} %fusion.6, f32[4,64,128,8]{2,1,3,0:T(8,128)S(1)} %convolution_bitcast_fusion.3, pred[8,8]{1,0:T(8,128)(4,1)S(1)} %copy-done.32), kind=kOutput, calls=%fused_computation.83 | convolution fusion | flops 25276416 | bytes 2129984 | tf_op jit(solution)/shard_map/transpose(jvp(hnmk,mhkv->nhkv))/dot_general | solution.py:25
  130.1 3.7 %pad_add_fusion = (f32[4,8,64,64]{2,3,1,0:T(8,128)}, bf16[4,8,64,64]{2,3,1,0:T(8,128)(2,1)}, bf16[4,8,64,64]{2,3,1,0:T(8,128)(2,1)S(1)}) fusion(f32[4,8,1,64]{2,3,1,0:T(8,128)S(1)} %fusion.3, f32[4,8,64,64]{2,3,1,0:T(8,128)S(1)} %fusion.44, f32[4,8,64,64]{2,1,3,0:T(8,128)S(1)} %mul.72, f32[4,8,64,64]{2,3,1,0:T(8,128)S(1)} %copy.195, ...), kind=kOutput, calls=%fused_computation.22 | convolution fusion | flops 103677952 | bytes 4734976 | tf_op jit(solution)/shard_map/transpose(jvp(hnik,hnjk->hnij))/dot_general | solution.py:43
  138.8 4.8 %all-to-all-start.4 = ((bf16[4,128,256]{1,2,0:T(8,128)(2,1)}), bf16[4,128,256]{1,2,0:T(8,128)(2,1)S(1)}, u32[]{:S(2)}, u32[]{:S(2)}) async-start(bf16[4,128,256]{1,2,0:T(8,128)(2,1)} %copy.213), calls=%async_computation.4 | async-start | bytes 524288 | tf_op jit(solution)/shard_map/all_to_all | solution.py:103
  143.6 3.1 %convolution_select_fusion.2 = f32[4,8,64,64]{3,2,1,0:T(8,128)} fusion(pred[64,64]{1,0:T(8,128)(4,1)S(1)} %copy-done.28, f32[4,8,64,64]{2,1,3,0:T(8,128)S(1)} %reshape.166, f32[4,8,64,64]{2,3,1,0:T(8,128)S(1)} %copy.195, f32[4,8,64,64]{2,1,3,0:T(8,128)S(1)} %mul.72), kind=kOutput, calls=%fused_computation.11 | convolution fusion | flops 101187584 | bytes 2101248 | tf_op jit(solution)/shard_map/jvp(hnik,hnjk->hnij)/dot_general | solution.py:43
  148.3 3.2 %fusion.11 = f32[4,8,64,128]{3,2,1,0:T(8,128)S(1)} fusion(f32[4,8,64,64]{2,3,1,0:T(8,128)S(1)} %copy-done.4, f32[8,4,64,128]{3,0,2,1:T(8,128)} %copy-done.9), kind=kOutput, calls=%fused_computation.30 | convolution fusion | flops 201326592 | bytes 2621440 | tf_op jit(solution)/shard_map/transpose(jvp(hnjk,hnjv->nhkv))/dot_general | solution.py:48
  151.5 5.2 %all-to-all-start.6 = ((bf16[4,128,256]{1,2,0:T(8,128)(2,1)}), bf16[4,128,256]{1,2,0:T(8,128)(2,1)S(1)}, u32[]{:S(2)}, u32[]{:S(2)}) async-start(bf16[4,128,256]{1,2,0:T(8,128)(2,1)} %copy.226), calls=%async_computation.6 | async-start | bytes 524288 | tf_op jit(solution)/shard_map/all_to_all | solution.py:106
  159.6 25.8 %fusion.47 = f32[4,8,64,64]{3,1,2,0:T(8,128)S(1)} fusion(f32[4,8,64,64]{3,1,2,0:T(8,128)S(1)} %copy.246), kind=kOutput, calls=%fused_computation.85 | output fusion | flops 8257536 | bytes 1048576 | tf_op jit(solution)/shard_map/transpose(jvp(jit(cumsum)))/reduce_window_sum | solution.py:36
  186.1 5.2 %all-to-all-start.7 = ((bf16[4,128,512]{2,1,0:T(8,128)(2,1)}), bf16[4,128,512]{2,1,0:T(8,128)(2,1)S(1)}, u32[]{:S(2)}, u32[]{:S(2)}) async-start(bf16[4,128,512]{2,1,0:T(8,128)(2,1)} %convert_element_type.84), calls=%async_computation.7 | async-start | bytes 1048576 | tf_op jit(solution)/shard_map/all_to_all | solution.py:109
  193.9 56.5 %all-reduce.3.cloned.1.call-done = f32[64,256]{1,0:T(8,128)} async-done(((f32[64,256]{1,0:T(8,128)}), f32[64,256]{1,0:T(8,128)}) %all-reduce.3.cloned.1.call-update) | async-done | bytes 65552 | tf_op jit(solution)/shard_map/psum | solution.py:124
  250.4 14.1 %all_gather.7 = f32[64,1024]{1,0:T(8,128)S(1)} all-gather(f32[64,256]{1,0:T(8,128)} %all-reduce.3.cloned.1.call-done), channel_id=1, replica_groups=mesh['sp'=4,'dp'=8] {'sp'}, dimensions={1}, use_global_device_ids=true | all-gather | bytes 327680 | tf_op jit(solution)/shard_map/all_gather | solution.py:125
  (140 shorter events, 51.1 us)
Async XLA Ops:
  8.0 41.7 %copy-start = (bf16[64,1024]{1,0:T(8,128)(2,1)S(1)}, bf16[64,1024]{1,0:T(8,128)(2,1)}, u32[]{:S(2)}) copy-start(bf16[64,1024]{1,0:T(8,128)(2,1)} %param.13) | copy-start | bytes 393220
  8.0 12.1 %all-to-all-start.1 = ((bf16[128,4,4]{0,2,1:T(4,128)(2,1)}), bf16[128,4,4]{0,2,1:T(4,128)(2,1)S(1)}, u32[]{:S(2)}, u32[]{:S(2)}) async-start(bf16[128,4,4]{0,2,1:T(4,128)(2,1)} %bitcast.169), calls=%async_computation.1 | async-start | bytes 8192 | tf_op jit(solution)/shard_map/all_to_all | solution.py:77
  20.1 3.6 %copy-start.20 = (bf16[128,1024]{1,0:T(8,128)(2,1)S(1)}, bf16[128,1024]{1,0:T(8,128)(2,1)}, u32[]{:S(2)}) copy-start(bf16[128,1024]{1,0:T(8,128)(2,1)} %param.9) | copy-start | bytes 786436
  20.1 11.4 %all-to-all-start.5 = ((bf16[128,4,256]{0,2,1:T(8,128)(2,1)}), bf16[128,4,256]{0,2,1:T(8,128)(2,1)S(1)}, u32[]{:S(2)}, u32[]{:S(2)}) async-start(bf16[128,4,256]{0,2,1:T(8,128)(2,1)} %bitcast.24), calls=%async_computation.5 | async-start | bytes 524288 | tf_op jit(solution)/shard_map/all_to_all | solution.py:73
  23.6 11.3 %copy-start.17 = (bf16[128,2048]{1,0:T(8,128)(2,1)S(1)}, bf16[128,2048]{1,0:T(8,128)(2,1)}, u32[]{:S(2)}) copy-start(bf16[128,2048]{1,0:T(8,128)(2,1)} %param.11) | copy-start | bytes 1572868
  31.5 19.5 %all-to-all-start = ((bf16[128,4,256]{0,2,1:T(8,128)(2,1)}), bf16[128,4,256]{0,2,1:T(8,128)(2,1)S(1)}, u32[]{:S(2)}, u32[]{:S(2)}) async-start(bf16[128,4,256]{0,2,1:T(8,128)(2,1)} %bitcast), calls=%async_computation | async-start | bytes 524288 | tf_op jit(solution)/shard_map/all_to_all | solution.py:74
  49.0 1.9 copy-start.21
  51.0 5.4 %copy-start.18 = (bf16[128,2048]{1,0:T(8,128)(2,1)S(1)}, bf16[128,2048]{1,0:T(8,128)(2,1)}, u32[]{:S(2)}) copy-start(bf16[128,2048]{1,0:T(8,128)(2,1)} %param.10) | copy-start | bytes 1572868
  51.7 32.2 %all-to-all-start.3 = ((bf16[128,4,512]{2,0,1:T(8,128)(2,1)}), bf16[128,4,512]{2,0,1:T(8,128)(2,1)}, u32[]{:S(2)}, u32[]{:S(2)}) async-start(bf16[128,4,512]{2,0,1:T(8,128)(2,1)} %bitcast.143), calls=%async_computation.3 | async-start | bytes 1048576 | tf_op jit(solution)/shard_map/all_to_all | solution.py:76
  83.9 15.5 %all-to-all-start.2 = ((bf16[128,4,512]{2,0,1:T(8,128)(2,1)}), bf16[128,4,512]{2,0,1:T(8,128)(2,1)}, u32[]{:S(2)}, u32[]{:S(2)}) async-start(bf16[128,4,512]{2,0,1:T(8,128)(2,1)} %bitcast.144), calls=%async_computation.2 | async-start | bytes 1048576 | tf_op jit(solution)/shard_map/all_to_all | solution.py:75
  102.5 7.0 %copy-start.5 = (bf16[4,512,128]{2,1,0:T(8,128)(2,1)}, bf16[4,512,128]{2,1,0:T(8,128)(2,1)S(1)}, u32[]{:S(2)}) copy-start(bf16[4,512,128]{2,1,0:T(8,128)(2,1)S(1)} %copy.198) | copy-start | bytes 1572868
  106.6 2.9 %copy-start.9 = (f32[8,4,64,128]{3,0,2,1:T(8,128)}, f32[8,4,64,128]{3,0,2,1:T(8,128)S(1)}, u32[]{:S(2)}) copy-start(f32[8,4,64,128]{3,0,2,1:T(8,128)S(1)} %convolution_bitcast_fusion) | copy-start | bytes 3145732
  117.3 2.0 copy-start.26
  126.7 1.8 copy-start.13
  138.8 4.8 %copy-start.28 = (pred[64,64]{1,0:T(8,128)(4,1)S(1)}, pred[64,64]{1,0:T(8,128)(4,1)}, u32[]{:S(2)}) copy-start(pred[64,64]{1,0:T(8,128)(4,1)} %iota_compare_fusion) | copy-start | bytes 12292
  138.8 12.7 %all-to-all-start.4 = ((bf16[4,128,256]{1,2,0:T(8,128)(2,1)}), bf16[4,128,256]{1,2,0:T(8,128)(2,1)S(1)}, u32[]{:S(2)}, u32[]{:S(2)}) async-start(bf16[4,128,256]{1,2,0:T(8,128)(2,1)} %copy.213), calls=%async_computation.4 | async-start | bytes 524288 | tf_op jit(solution)/shard_map/all_to_all | solution.py:103
  143.6 3.1 %copy-start.14 = (bf16[4,8,64,64]{2,3,1,0:T(8,128)(2,1)S(1)}, bf16[4,8,64,64]{2,3,1,0:T(8,128)(2,1)}, u32[]{:S(2)}) copy-start(bf16[4,8,64,64]{2,3,1,0:T(8,128)(2,1)} %get-tuple-element.23) | copy-start | bytes 786436
  148.3 8.4 %copy-start.6 = (f32[4,8,64,64]{3,2,1,0:T(8,128)S(1)}, f32[4,8,64,64]{3,2,1,0:T(8,128)}, u32[]{:S(2)}) copy-start(f32[4,8,64,64]{3,2,1,0:T(8,128)} %convolution_select_fusion.2) | copy-start | bytes 1572868
  151.5 5.3 %copy-start.2 = (bf16[4,512,128]{2,1,0:T(8,128)(2,1)S(1)}, bf16[4,512,128]{2,1,0:T(8,128)(2,1)}, u32[]{:S(2)}) copy-start(bf16[4,512,128]{2,1,0:T(8,128)(2,1)} %copy.205) | copy-start | bytes 1572868
  151.5 34.6 %all-to-all-start.6 = ((bf16[4,128,256]{1,2,0:T(8,128)(2,1)}), bf16[4,128,256]{1,2,0:T(8,128)(2,1)S(1)}, u32[]{:S(2)}, u32[]{:S(2)}) async-start(bf16[4,128,256]{1,2,0:T(8,128)(2,1)} %copy.226), calls=%async_computation.6 | async-start | bytes 524288 | tf_op jit(solution)/shard_map/all_to_all | solution.py:106
  186.1 5.3 %copy-start.19 = (f32[256,512]{1,0:T(8,128)S(1)}, f32[256,512]{1,0:T(8,128)}, u32[]{:S(2)}) copy-start(f32[256,512]{1,0:T(8,128)} %get-tuple-element.30) | copy-start | bytes 1572868
  186.1 81.5 %all-to-all-start.7 = ((bf16[4,128,512]{2,1,0:T(8,128)(2,1)}), bf16[4,128,512]{2,1,0:T(8,128)(2,1)S(1)}, u32[]{:S(2)}, u32[]{:S(2)}) async-start(bf16[4,128,512]{2,1,0:T(8,128)(2,1)} %convert_element_type.84), calls=%async_computation.7 | async-start | bytes 1048576 | tf_op jit(solution)/shard_map/all_to_all | solution.py:109
  191.3 59.1 %all-reduce.3.cloned.1.call-start = ((), (), s32[]{:S(2)}) async-start(), calls=%async_computation.10 | async-start | bytes 131072 | tf_op jit(solution)/shard_map/psum | solution.py:124
  193.0 71.5 %reduce-scatter.2.cloned.1.call-start = ((), (), s32[]{:S(2)}) async-start(), calls=%async_computation.9 | async-start | bytes 163840 | tf_op jit(solution)/shard_map/reduce_scatter | solution.py:118
  (19 other events, 22.7 us)
Sparse Core Ops, SparseCore 0:
  195.7 54.6 all-reduce.2
Sparse Core Ops, SparseCore 1:
  196.3 20.9 reduce-scatter.1
where the time goes:
time: 279 us; the launch traced here: 277 us
  waiting for transfers between devices  67.7 us (24%)
  other arithmetic  56 us (20%)
  local copies, waits for them, and re-layouts  39.8 us (14%)
  starting transfers between devices  38 us (14%)
  matrix products  32.9 us (12%)
  blocking collectives  26.6 us (10%)
  between operations  15.9 us (6%)
    psum x1, waiting for transfers between devices, on_device(): summed = lax.psum(local_weight, 'dp')  56.5 us
    another operation x2, other arithmetic, gla_forward(): cumulative = jnp.cumsum(blocked(logarithm_decay), axis=2)  51.6 us
    all_gather x1, blocking collectives, on_device(): weight_grad = lax.all_gather(summed, 'sp', axis=1, tiled=True)  14.1 us
    all_gather x1, blocking collectives, on_device(): hidden_code_rows = lax.all_gather(compact_factor, 'sp', axis=0, tiled=True)  12.5 us
    unnamed x72, local copies, waits for them, and re-layouts  10.3 us
    dot_general x3, matrix products, carry_states(): return jnp.einsum('hnmk,mhkv->nhkv', weights, increments, precision=highest)  9.75 us
    dot_general x3, matrix products, gla_forward(): jnp.einsum('hnik,hnjk->hnij', query_decayed, key_inverse, precision=highest)  8.12 us
    all_to_all x1, waiting for transfers between devices, on_device(): lax.all_to_all(probe_vectors, 'sp', split_axis=1, concat_axis=0, tiled=True)  7.02 us
  transfers between devices with their start and end apart: 10, of which 4 were waited for; matrix products, arithmetic and copies ran while one was open for 31% of the time, Pallas kernels for 0%

commit v1 on v0

v1 whole, which is shorter than its diff:
```python
import functools

import jax
import jax.numpy as jnp
from jax import lax
from jax.experimental import pallas as pl
from jax.experimental.pallas import tpu as pltpu
from jax.sharding import PartitionSpec as P

KEY = 64
VAL = 128
LANES = 128
BLOCK = 64
GATE_NORM = 16.0
SCALE = KEY ** (-0.5)
F32 = jnp.float32
BF16 = jnp.bfloat16

NN = (((1,), (0,)), ((), ()))
NT = (((1,), (1,)), ((), ()))
TN = (((0,), (0,)), ((), ()))


def dot(a, b, dims=NN):
    return lax.dot_general(a, b, dims, preferred_element_type=F32)


def split(x, parts):
    pieces = []
    for _ in range(parts):
        piece = x.astype(BF16)
        pieces.append(piece)
        x = x - piece.astype(F32)
    return pieces


def triangle(rows, keep):
    r = lax.broadcasted_iota(jnp.int32, (rows, rows), 0)
    c = lax.broadcasted_iota(jnp.int32, (rows, rows), 1)
    return jnp.where(keep(r, c), 1.0, 0.0).astype(BF16)


def first_head(shape):
    return lax.broadcasted_iota(jnp.int32, shape, 1) < KEY


def pick(a, b):
    return jnp.where(first_head(a.shape), a, b)


def lanes(p):
    return slice(p * LANES, (p + 1) * LANES)


def value_lanes(h):
    return slice(h * VAL, (h + 1) * VAL)


def gates_kernel(q, k, v, do, c, w, b, spike, st, rt, cum_ref, sig_ref, qs_ref, kd_ref):
    rows, width = q.shape
    heads = spike.shape[1]
    logit = dot(c[...], w[...]) + b[...]
    small = jnp.exp(-jnp.abs(logit))
    log_sig = jnp.minimum(logit, 0.0) - jnp.log1p(small)
    sig_ref[...] = jnp.where(logit >= 0.0, small, 1.0) / ((1.0 + small) * GATE_NORM)
    owner = lax.broadcasted_iota(jnp.int32, (heads, width), 1) // KEY
    head = lax.broadcasted_iota(jnp.int32, (heads, width), 0)
    spread = jnp.where(owner == head, 1.0, 0.0).astype(BF16)
    log_decay = log_sig / GATE_NORM + dot(spike[...], spread)
    lower = triangle(rows, lambda r, s: r >= s)
    cum = sum(dot(lower, piece) for piece in split(log_decay, 3))
    cum_ref[...] = cum
    total = cum[rows - 1 :, :]
    qs = (q[...].astype(F32) * (SCALE * jnp.exp(cum))).astype(BF16)
    kd = (k[...].astype(F32) * jnp.exp(total - cum)).astype(BF16)
    qs_ref[...] = qs
    kd_ref[...] = kd
    for p in range(width // LANES):
        both = slice(2 * p * VAL, 2 * (p + 1) * VAL)
        s_pair = dot(v[:, both], kd[:, lanes(p)], TN)
        st[:, lanes(p)] = pick(s_pair[:VAL], s_pair[VAL:]).astype(BF16)
        r_pair = dot(do[:, both], qs[:, lanes(p)], TN)
        rt[:, lanes(p)] = pick(r_pair[:VAL], r_pair[VAL:]).astype(BF16)


def inner_kernel(q, k, v, do, cum_ref, dq, dk, dv, dec):
    rows, width = q.shape
    upper = triangle(rows, lambda r, s: r <= s)
    r = lax.broadcasted_iota(jnp.int32, (rows, rows), 0)
    s = lax.broadcasted_iota(jnp.int32, (rows, rows), 1)
    causal = r >= s
    causal_t = r <= s
    for p in range(width // LANES):
        cum = cum_ref[:, lanes(p)]
        middle = cum[BLOCK - 1 : BLOCK, :]
        q_up = SCALE * jnp.exp(cum - middle)
        k_up = jnp.exp(middle - cum)
        qa = (q[:, lanes(p)].astype(F32) * q_up).astype(BF16)
        ka = (k[:, lanes(p)].astype(F32) * k_up).astype(BF16)
        zero = jnp.zeros_like(ka)
        grads = []
        for j in range(2):
            h = 2 * p + j
            own = first_head(ka.shape) if j == 0 else jnp.logical_not(first_head(ka.shape))
            vj = v[:, value_lanes(h)]
            doj = do[:, value_lanes(h)]
            at = jnp.where(causal_t, dot(jnp.where(own, ka, zero), qa, NT), 0.0).astype(BF16)
            dv[:, value_lanes(h)] = dot(at, doj)
            g = jnp.where(causal, dot(doj, vj, NT), 0.0).astype(BF16)
            gt = jnp.where(causal_t, dot(vj, doj, NT), 0.0).astype(BF16)
            grads.append((dot(g, ka), dot(gt, qa)))
        dqa = pick(grads[0][0], grads[1][0])
        dka = pick(grads[0][1], grads[1][1])
        dq[:, lanes(p)] = dqa * q_up
        dk[:, lanes(p)] = dka * k_up
        flow = qa.astype(F32) * dqa - ka.astype(F32) * dka
        dec[:, lanes(p)] = sum(dot(upper, piece) for piece in split(flow, 3))


def carried(x, state, p):
    return pick(
        dot(x[:, value_lanes(2 * p)], state[:, lanes(p)]),
        dot(x[:, value_lanes(2 * p + 1)], state[:, lanes(p)]),
    )


def weight_kernel(v, do, c, cum_ref, sig_ref, qs, kd, dec, st, rt, gate, wg):
    rows, width = qs.shape
    upper = triangle(rows, lambda r, s: r <= s)
    before = triangle(rows, lambda r, s: r > s)
    for p in range(width // LANES):
        sp, rp = st[:, lanes(p)], rt[:, lanes(p)]
        t2 = qs[:, lanes(p)].astype(F32) * carried(do, st, p)
        t3 = kd[:, lanes(p)].astype(F32) * carried(v, rt, p)
        meet = jnp.sum(sp.astype(F32) * rp.astype(F32), axis=0, keepdims=True)
        total = jnp.exp(cum_ref[rows - 1 :, lanes(p)]) * meet + dec[:, lanes(p)]
        total += sum(dot(upper, piece) for piece in split(t2, 3))
        total += sum(dot(before, piece) for piece in split(t3, 3))
        g = (total * sig_ref[:, lanes(p)]).astype(BF16)
        gate[:, lanes(p)] = g
        wg[:, lanes(p)] = dot(c[...], g, TN)


def finish_kernel(v, do, w, cum_ref, kd, dq_in, dk_in, dv_in, st, rt, gate, dq, dk, dv, lat):
    rows, width = kd.shape
    lat[...] = dot(gate[...], w[...], NT).astype(BF16)
    for p in range(width // LANES):
        cum = cum_ref[:, lanes(p)]
        total = cum[rows - 1 :, :]
        dq[:, lanes(p)] = (
            dq_in[:, lanes(p)] + carried(do, st, p) * (SCALE * jnp.exp(cum))
        ).astype(BF16)
        dk[:, lanes(p)] = (
            dk_in[:, lanes(p)] + carried(v, rt, p) * jnp.exp(total - cum)
        ).astype(BF16)
        kp = kd[:, lanes(p)]
        zero = jnp.zeros_like(kp)
        for j in range(2):
            h = 2 * p + j
            own = first_head(kp.shape) if j == 0 else jnp.logical_not(first_head(kp.shape))
            add = dot(jnp.where(own, kp, zero), rt[:, lanes(p)], NT)
            dv[:, value_lanes(h)] = (dv_in[:, value_lanes(h)] + add).astype(BF16)


def call(kernel, outs, flops, *args):
    moved = sum(a.size * a.dtype.itemsize for a in args)
    return pl.pallas_call(
        kernel,
        out_shape=[jax.ShapeDtypeStruct(s, d) for s, d in outs],
        compiler_params=pltpu.CompilerParams(vmem_limit_bytes=24 * 1024 * 1024),
        cost_estimate=pl.CostEstimate(flops=flops, bytes_accessed=moved, transcendentals=0),
        name=kernel.__name__,
    )(*args)


def swap(x, axis, size, bit):
    return lax.ppermute(x, axis, [(i, i ^ bit) for i in range(size)])


def add_over(x, axis, size, low):
    bit = low
    while bit < size:
        x = x.astype(BF16)
        if 2 * bit < size:
            one, two, three = (swap(x, axis, size, m * bit) for m in (1, 2, 3))
            x = (x.astype(F32) + one.astype(F32)) + (two.astype(F32) + three.astype(F32))
            bit *= 4
        else:
            x = x.astype(F32) + swap(x, axis, size, bit).astype(F32)
            bit *= 2
    return x


def exchange(st, rt, decay, n, ndp):
    me = lax.axis_index("sp")
    left = jnp.zeros_like(st)
    right = jnp.zeros_like(rt)
    for step in range(n - 1):
        mirror = n - 1 - step
        forward = st.astype(F32) + decay * left.astype(F32)
        backward = rt.astype(F32) + decay * right.astype(F32)
        message = jnp.where(me == step, forward, backward).astype(BF16)
        partner = {}
        for a, b in ((step, step + 1), (mirror, mirror - 1)):
            partner[a] = b
        for a, b in list(partner.items()):
            partner.setdefault(b, a)
        whole = all(partner.get(b) == a for a, b in partner.items())
        pairs = []
        for i in range(n):
            for d in range(ndp):
                if i in partner:
                    pairs.append((i * ndp + d, partner[i] * ndp + d))
                elif ndp % 2 == 0:
                    pairs.append((i * ndp + d, i * ndp + (d ^ 1)))
        if not whole:
            pairs = [
                (a * ndp + d, b * ndp + d)
                for a, b in ((step, step + 1), (mirror, mirror - 1))
                for d in range(ndp)
            ]
        got = lax.ppermute(message, ("sp", "dp"), pairs)
        left = jnp.where(me == step + 1, got, left)
        right = jnp.where(me == mirror - 1, got, right)
    return left, right


def on_device(n, ndp, q, k, v, do, c, w, b, spike):
    rows, width = q.shape
    rank = c.shape[1]
    wide = v.shape[1]
    square = 2 * rows * wide * rows
    st, rt, cum, sig, qs, kd = call(
        gates_kernel,
        [((VAL, width), BF16)] * 2
        + [((rows, width), F32)] * 2
        + [((rows, width), BF16)] * 2,
        2 * square,
        q, k, v, do, c, w, b.reshape(1, width), spike,
    )
    dq_in, dk_in, dv_in, dec = call(
        inner_kernel,
        [((rows, width), F32)] * 2 + [((rows, wide), F32), ((rows, width), F32)],
        6 * square,
        q, k, v, do, cum,
    )
    decay = jnp.exp(cum[rows - 1 :, :])
    left, right = exchange(st, rt, decay, n, ndp)
    gate, part = call(
        weight_kernel,
        [((rows, width), BF16), ((rank, width), F32)],
        3 * square,
        v, do, c, cum, sig, qs, kd, dec, left, right,
    )
    dq, dk, dv, lat = call(
        finish_kernel,
        [((rows, width), BF16)] * 2 + [((rows, wide), BF16), ((rows, rank), BF16)],
        4 * square,
        v, do, w, cum, kd, dq_in, dk_in, dv_in, left, right, gate,
    )
    half = rank // 2
    odd = lax.axis_index("dp") % 2 == 1
    mine = jnp.where(odd, part[half:], part[:half])
    other = jnp.where(odd, part[:half], part[half:])
    mine = mine + swap(other, "dp", ndp, 1)
    mine = add_over(mine, "dp", ndp, 2)
    mine = add_over(mine, "sp", n, 1)
    other = swap(mine, "dp", ndp, 1)
    weight = jnp.concatenate([jnp.where(odd, other, mine), jnp.where(odd, mine, other)], axis=0)
    return dq, dk, dv, lat, weight


def solution(mesh):
    token = P(("dp", "sp"), None)
    return jax.shard_map(
        functools.partial(on_device, mesh.shape["sp"], mesh.shape["dp"]),
        mesh=mesh,
        in_specs=(token, token, token, token, token, P(), P(), token),
        out_specs=(token, token, token, token, P()),
        check_vma=False,
    )
```

time: 279 us -> 60.9 us (0.22)
  other arithmetic: 56 us -> 3.18 us
  waiting for transfers between devices: 67.7 us -> 16.7 us
  matrix products: 32.9 us -> 0 us
  local copies, waits for them, and re-layouts: 39.8 us -> 9.26 us
  blocking collectives: 26.6 us -> 0 us
  starting transfers between devices: 38 us -> 18.7 us
  between operations: 15.9 us -> 0.88 us
  Pallas kernels: 0 us -> 11.8 us
    psum x1 -> x0, waiting for transfers between devices: 56.5 us -> none  [on_device(): summed = lax.psum(local_weight, 'dp')]
    another operation x4 -> x0, other arithmetic: 53.1 us -> none  [the longest x2 51.6 us: gla_forward(): cumulative = jnp.cumsum(blocked(logarithm_decay), axis=2)]
    all_to_all x8 -> x0, starting transfers between devices: 37.9 us -> none  [the longest x1 6.49 us: on_device(): lax.all_to_all(surplus_damping, 'sp', split_axis=1, concat_axis=0, tiled=...]
    dot_general x16 -> x0, matrix products: 32.9 us -> none  [the longest x3 9.75 us: carry_states(): return jnp.einsum('hnmk,mhkv->nhkv', weights, increments, precision=highest)]
    all_gather x2 -> x0, blocking collectives: 26.6 us -> none  [the longest x1 14.1 us: on_device(): weight_grad = lax.all_gather(summed, 'sp', axis=1, tiled=True)]
    ppermute x0 -> x11, starting transfers between devices: none -> 18.7 us  [the longest x3 10.5 us: exchange(): got = lax.ppermute(message, ('sp', 'dp'), pairs)]
    ppermute x0 -> x11, waiting for transfers between devices: none -> 16.7 us  [the longest x8 8.86 us: swap(): return lax.ppermute(x, axis, [(i, i ^ bit) for i in range(size)])]
    pallas_call x0 -> x4, Pallas kernels: none -> 11.8 us  [call(): pl.pallas_call(kernel, out_shape=[jax.ShapeDtypeStruct(s, d) for s, d in...]
  transfers between devices with their start and end apart: 10 -> 11, of which waited for: 4 -> 8; matrix products, arithmetic and copies ran while one was open for 31% -> 1% of each run, Pallas kernels for 0% -> 12%
where the time goes in v1:
time: 60.9 us; the launch traced here: 60.4 us
  starting transfers between devices  18.7 us (31%)
  waiting for transfers between devices  16.7 us (27%)
  Pallas kernels  11.8 us (19%)
  local copies, waits for them, and re-layouts  9.26 us (15%)
  other arithmetic  3.18 us (5%)
  between operations  0.88 us (1%)
    pallas_call x4, Pallas kernels, call(): pl.pallas_call(kernel, out_shape=[jax.ShapeDtypeStruct(s, d) for s, d in...  11.8 us
    ppermute x3, starting transfers between devices, exchange(): got = lax.ppermute(message, ('sp', 'dp'), pairs)  10.5 us
    unnamed x39, local copies, waits for them, and re-layouts  9.24 us
    ppermute x8, waiting for transfers between devices, swap(): return lax.ppermute(x, axis, [(i, i ^ bit) for i in range(size)])  8.86 us
    ppermute x8, starting transfers between devices, swap(): return lax.ppermute(x, axis, [(i, i ^ bit) for i in range(size)])  8.15 us
    ppermute x3, waiting for transfers between devices, exchange(): got = lax.ppermute(message, ('sp', 'dp'), pairs)  7.82 us
    convert_element_type x3, other arithmetic, exchange(): message = jnp.where(me == step, forward, backward).astype(BF16)  2.26 us
  transfers between devices with their start and end apart: 11, of which 8 were waited for; matrix products, arithmetic and copies ran while one was open for 1% of the time, Pallas kernels for 12%

profile of v1, /device:TPU:0, one launch (start us, length us, event | category | flops | bytes accessed | tf_op | source)
XLA Modules:
  0.0 60.4 jit_solution(2353376395929337722)
XLA Ops:
  0.6 0.8 %copy.13.c = bf16[128,64]{1,0:T(8,128)(2,1)S(1)} copy(bf16[128,64]{0,1:T(8,128)(2,1)} %param.12) | data formatting | bytes 32768 | tf_op args[4]
  2.2 1.0 %copy-done = bf16[128,2048]{1,0:T(8,128)(2,1)S(1)} copy-done((bf16[128,2048]{1,0:T(8,128)(2,1)S(1)}, bf16[128,2048]{1,0:T(8,128)(2,1)}, u32[]{:S(2)}) %copy-start) | copy-done | bytes 524312
  3.2 1.0 %copy-done.2 = bf16[128,2048]{1,0:T(8,128)(2,1)S(1)} copy-done((bf16[128,2048]{1,0:T(8,128)(2,1)S(1)}, bf16[128,2048]{1,0:T(8,128)(2,1)}, u32[]{:S(2)}) %copy-start.2) | copy-done | bytes 524312
  4.3 0.9 %copy-done.4 = bf16[128,1024]{1,0:T(8,128)(2,1)S(1)} copy-done((bf16[128,1024]{1,0:T(8,128)(2,1)S(1)}, bf16[128,1024]{1,0:T(8,128)(2,1)}, u32[]{:S(2)}) %copy-start.4) | copy-done | bytes 262168
  5.2 0.9 %copy-done.6 = bf16[128,1024]{1,0:T(8,128)(2,1)S(1)} copy-done((bf16[128,1024]{1,0:T(8,128)(2,1)S(1)}, bf16[128,1024]{1,0:T(8,128)(2,1)}, u32[]{:S(2)}) %copy-start.6) | copy-done | bytes 262168
  6.2 0.9 %copy-done.8 = bf16[64,1024]{1,0:T(8,128)(2,1)S(1)} copy-done((bf16[64,1024]{1,0:T(8,128)(2,1)S(1)}, bf16[64,1024]{1,0:T(8,128)(2,1)}, u32[]{:S(2)}) %copy-start.8) | copy-done | bytes 131096
  7.1 1.4 %gates_kernel.1 = (bf16[128,1024]{1,0:T(8,128)(2,1)S(1)}, bf16[128,1024]{1,0:T(8,128)(2,1)S(1)}, f32[128,1024]{1,0:T(8,128)S(1)}, f32[128,1024]{1,0:T(8,128)S(1)...) custom-call(bf16[128,1024]{1,0:T(8,128)(2,1)S(1)} %copy-done.4, bf16[128,1024]{1,0:T(8,128)(2,1)S(1)} %copy-done.6, ...), custom_call_target="tpu_custom_call" | custom-call | flops 134217728 | bytes 1728512 | tf_op jit(solution)/shard_map/gates_kernel/pallas_call | solution.py:167
  9.2 3.1 %collective-permute-start = (bf16[128,1024]{1,0:T(8,128)(2,1)S(1)}, bf16[128,1024]{1,0:T(8,128)(2,1)S(1)}, u32[]{:S(2)}, u32[]{:S(2)}) collective-permute-start(bf16[128,1024]{1,0:T(8,128)(2,1)S(1)} %fusion.1), channel_id=1, source_target_pairs={{0,8},{1,9},{2,10},{3,11},{4,12},{5,13},{6,14},{7,15},{8,0},{9,1},... | collective-permute-start | bytes 786440 | tf_op jit(solution)/shard_map/ppermute | solution.py:222
  12.2 6.3 %collective-permute-done = bf16[128,1024]{1,0:T(8,128)(2,1)S(1)} collective-permute-done((bf16[128,1024]{1,0:T(8,128)(2,1)S(1)}, bf16[128,1024]{1,0:T(8,128)(2,1)S(1)}, u32[]{:S(2)}, u32[]{:S(2)}) %collective-permute-start) | collective-permute-done | bytes 262176 | tf_op jit(solution)/shard_map/ppermute | solution.py:222
  19.5 1.5 %collective-permute-done.1 = bf16[128,1024]{1,0:T(8,128)(2,1)S(1)} collective-permute-done((bf16[128,1024]{1,0:T(8,128)(2,1)S(1)}, bf16[128,1024]{1,0:T(8,128)(2,1)S(1)}, u32[]{:S(2)}, u32[]{:S(2)}) %collective-permute-start.1) | collective-permute-done | bytes 262176 | tf_op jit(solution)/shard_map/ppermute | solution.py:222
  21.1 2.0 %fusion.5 = bf16[128,1024]{1,0:T(8,128)(2,1)} fusion(bf16[128,1024]{1,0:T(8,128)(2,1)S(1)} %get-tuple-element.26, bf16[128,1024]{1,0:T(8,128)(2,1)S(1)} %get-tuple-element.27, f32[1024]{0:T(1024)S(1)} %bitcast.5, pred[]{:T(512)S(6)} %eq.23, bf16[128,1024]{1,0:T(8,128)(2,1)S(1)} %collective-permute-done.1, bf16[128,1024]{1,0:T(8,128)(2,1)} %copy-done.13, ...), kind=kLoop, calls=%fused_computation.11 | loop fusion | flops 1835008 | bytes 1314818 | tf_op jit(solution)/shard_map/convert_element_type | solution.py:202
  23.0 7.4 %collective-permute-start.2 = (bf16[128,1024]{1,0:T(8,128)(2,1)}, bf16[128,1024]{1,0:T(8,128)(2,1)S(1)}, u32[]{:S(2)}, u32[]{:S(2)}) collective-permute-start(bf16[128,1024]{1,0:T(8,128)(2,1)} %fusion.5), channel_id=1, source_target_pairs={{0,8},{1,9},{2,10},{3,11},{4,12},{5,13},{6,14},{7,15},{8,0},{9,1},... | collective-permute-start | bytes 786440 | tf_op jit(solution)/shard_map/ppermute | solution.py:222
  30.5 5.3 %inner_kernel.1 = (f32[128,1024]{1,0:T(8,128)S(1)}, f32[128,1024]{1,0:T(8,128)S(1)}, f32[128,2048]{1,0:T(8,128)S(1)}, f32[128,1024]{1,0:T(8,128)S(1)}) custom-call(bf16[128,1024]{1,0:T(8,128)(2,1)S(1)} %copy-done.5, bf16[128,1024]{1,0:T(8,128)(2,1)S(1)} %copy-done.7, bf16[128,2048]{1,0:T(8,128)(2,1)S(1)} %copy-done.1, bf16[128,2048]{1,0:T(8,128)(2,1)S(1)} %copy-done.3, ...), custom_call_target="tpu_custom_call" | custom-call | flops 402653184 | bytes 2097152 | tf_op jit(solution)/shard_map/inner_kernel/pallas_call | solution.py:167
  35.9 0.8 %copy-done.11 = bf16[128,1024]{1,0:T(8,128)(2,1)S(1)} copy-done((bf16[128,1024]{1,0:T(8,128)(2,1)S(1)}, bf16[128,1024]{1,0:T(8,128)(2,1)}, u32[]{:S(2)}) %copy-start.11) | copy-done | bytes 262168
  36.7 3.3 %weight_kernel.1 = (bf16[128,1024]{1,0:T(8,128)(2,1)S(1)}, f32[64,1024]{1,0:T(8,128)S(1)}) custom-call(bf16[128,2048]{1,0:T(8,128)(2,1)S(1)} %copy-done.1, bf16[128,2048]{1,0:T(8,128)(2,1)S(1)} %copy-done.3, bf16[128,64]{1,0:T(8,128)(2,1)S(1)} %copy.13.c, f32[128,1024]{1,0:T(8,128)S(1)} %get-tuple-element.21.cum_ref, ...), custom_call_target="tpu_custom_call" | custom-call | flops 201326592 | bytes 3686400 | tf_op jit(solution)/shard_map/weight_kernel/pallas_call | solution.py:167
  40.1 1.3 %collective-permute-done.3 = f32[32,1024]{1,0:T(8,128)S(1)} collective-permute-done((f32[32,1024]{1,0:T(8,128)S(1)}, f32[32,1024]{1,0:T(8,128)S(1)}, u32[]{:S(2)}, u32[]{:S(2)}) %collective-permute-start.3) | collective-permute-done | bytes 131104 | tf_op jit(solution)/shard_map/ppermute | solution.py:177
  41.5 2.5 %collective-permute-start.6 = (bf16[32,1024]{1,0:T(8,128)(2,1)S(1)}, bf16[32,1024]{1,0:T(8,128)(2,1)S(1)}, u32[]{:S(2)}, u32[]{:S(2)}) collective-permute-start(bf16[32,1024]{1,0:T(8,128)(2,1)S(1)} %add_convert_fusion.1), channel_id=1, source_target_pairs={{0,6},{1,7},{2,4},{3,5},{4,2},{5,3},{6,0},{7,1},{8,14},{9,15},{10,... | collective-permute-start | bytes 196616 | tf_op jit(solution)/shard_map/ppermute | solution.py:177
  45.0 1.7 %collective-permute-done.6 = bf16[32,1024]{1,0:T(8,128)(2,1)S(1)} collective-permute-done((bf16[32,1024]{1,0:T(8,128)(2,1)S(1)}, bf16[32,1024]{1,0:T(8,128)(2,1)S(1)}, u32[]{:S(2)}, u32[]{:S(2)}) %collective-permute-start.6) | collective-permute-done | bytes 65568 | tf_op jit(solution)/shard_map/ppermute | solution.py:177
  46.7 1.5 %collective-permute-done.5 = bf16[32,1024]{1,0:T(8,128)(2,1)S(1)} collective-permute-done((bf16[32,1024]{1,0:T(8,128)(2,1)S(1)}, bf16[32,1024]{1,0:T(8,128)(2,1)S(1)}, u32[]{:S(2)}, u32[]{:S(2)}) %collective-permute-start.5) | collective-permute-done | bytes 65568 | tf_op jit(solution)/shard_map/ppermute | solution.py:177
  48.8 2.5 %collective-permute-start.9 = (bf16[32,1024]{1,0:T(8,128)(2,1)S(1)}, bf16[32,1024]{1,0:T(8,128)(2,1)S(1)}, u32[]{:S(2)}, u32[]{:S(2)}) collective-permute-start(bf16[32,1024]{1,0:T(8,128)(2,1)S(1)} %add_convert_fusion), channel_id=1, source_target_pairs={{0,24},{8,16},{16,8},{24,0},{1,25},{9,17},{17,9},{25,1},{2,26},{10... | collective-permute-start | bytes 196616 | tf_op jit(solution)/shard_map/ppermute | solution.py:177
  51.4 1.9 %collective-permute-start.7 = (bf16[32,1024]{1,0:T(8,128)(2,1)S(1)}, bf16[32,1024]{1,0:T(8,128)(2,1)S(1)}, u32[]{:S(2)}, u32[]{:S(2)}) collective-permute-start(bf16[32,1024]{1,0:T(8,128)(2,1)S(1)} %add_convert_fusion), channel_id=1, source_target_pairs={{0,8},{8,0},{16,24},{24,16},{1,9},{9,1},{17,25},{25,17},{2,10},{10... | collective-permute-start | bytes 196616 | tf_op jit(solution)/shard_map/ppermute | solution.py:177
  53.3 2.3 %collective-permute-done.9 = bf16[32,1024]{1,0:T(8,128)(2,1)S(1)} collective-permute-done((bf16[32,1024]{1,0:T(8,128)(2,1)S(1)}, bf16[32,1024]{1,0:T(8,128)(2,1)S(1)}, u32[]{:S(2)}, u32[]{:S(2)}) %collective-permute-start.9) | collective-permute-done | bytes 65568 | tf_op jit(solution)/shard_map/ppermute | solution.py:177
  55.6 1.4 %collective-permute-done.8 = bf16[32,1024]{1,0:T(8,128)(2,1)S(1)} collective-permute-done((bf16[32,1024]{1,0:T(8,128)(2,1)S(1)}, bf16[32,1024]{1,0:T(8,128)(2,1)S(1)}, u32[]{:S(2)}, u32[]{:S(2)}) %collective-permute-start.8) | collective-permute-done | bytes 65568 | tf_op jit(solution)/shard_map/ppermute | solution.py:177
  57.2 1.8 %finish_kernel.1 = (bf16[128,1024]{1,0:T(8,128)(2,1)}, bf16[128,1024]{1,0:T(8,128)(2,1)}, bf16[128,2048]{1,0:T(8,128)(2,1)}, bf16[128,64]{1,0:T(8,128)(2,1)S(1)}) custom-call(bf16[128,2048]{1,0:T(8,128)(2,1)S(1)} %copy-done.1, bf16[128,2048]{1,0:T(8,128)(2,1)S(1)} %copy-done.3, bf16[64,1024]{1,0:T(8,128)(2,1)S(1)} %copy-done.9, ...), custom_call_target="tpu_custom_call" | custom-call | flops 268435456 | bytes 4849664 | tf_op jit(solution)/shard_map/finish_kernel/pallas_call | solution.py:167
  (53 shorter events, 5.7 us)
Async XLA Ops:
  2.2 1.0 %copy-start = (bf16[128,2048]{1,0:T(8,128)(2,1)S(1)}, bf16[128,2048]{1,0:T(8,128)(2,1)}, u32[]{:S(2)}) copy-start(bf16[128,2048]{1,0:T(8,128)(2,1)} %v.7) | copy-start | bytes 1572868
  3.2 1.0 %copy-start.2 = (bf16[128,2048]{1,0:T(8,128)(2,1)S(1)}, bf16[128,2048]{1,0:T(8,128)(2,1)}, u32[]{:S(2)}) copy-start(bf16[128,2048]{1,0:T(8,128)(2,1)} %do.7) | copy-start | bytes 1572868
  4.3 0.9 %copy-start.4 = (bf16[128,1024]{1,0:T(8,128)(2,1)S(1)}, bf16[128,1024]{1,0:T(8,128)(2,1)}, u32[]{:S(2)}) copy-start(bf16[128,1024]{1,0:T(8,128)(2,1)} %q.3) | copy-start | bytes 786436
  5.2 0.9 %copy-start.6 = (bf16[128,1024]{1,0:T(8,128)(2,1)S(1)}, bf16[128,1024]{1,0:T(8,128)(2,1)}, u32[]{:S(2)}) copy-start(bf16[128,1024]{1,0:T(8,128)(2,1)} %k.3) | copy-start | bytes 786436
  9.2 9.3 %collective-permute-start = (bf16[128,1024]{1,0:T(8,128)(2,1)S(1)}, bf16[128,1024]{1,0:T(8,128)(2,1)S(1)}, u32[]{:S(2)}, u32[]{:S(2)}) collective-permute-start(bf16[128,1024]{1,0:T(8,128)(2,1)S(1)} %fusion.1), channel_id=1, source_target_pairs={{0,8},{1,9},{2,10},{3,11},{4,12},{5,13},{6,14},{7,15},{8,0},{9,1},... | collective-permute-start | bytes 786440 | tf_op jit(solution)/shard_map/ppermute | solution.py:222
  19.2 11.2 %copy-start.7 = (bf16[128,1024]{1,0:T(8,128)(2,1)S(1)}, bf16[128,1024]{1,0:T(8,128)(2,1)}, u32[]{:S(2)}) copy-start(bf16[128,1024]{1,0:T(8,128)(2,1)} %k.3) | copy-start | bytes 786436
  19.4 11.0 %copy-start.1 = (bf16[128,2048]{1,0:T(8,128)(2,1)S(1)}, bf16[128,2048]{1,0:T(8,128)(2,1)}, u32[]{:S(2)}) copy-start(bf16[128,2048]{1,0:T(8,128)(2,1)} %v.7) | copy-start | bytes 1572868
  19.4 11.0 %copy-start.3 = (bf16[128,2048]{1,0:T(8,128)(2,1)S(1)}, bf16[128,2048]{1,0:T(8,128)(2,1)}, u32[]{:S(2)}) copy-start(bf16[128,2048]{1,0:T(8,128)(2,1)} %do.7) | copy-start | bytes 1572868
  19.4 11.0 %copy-start.5 = (bf16[128,1024]{1,0:T(8,128)(2,1)S(1)}, bf16[128,1024]{1,0:T(8,128)(2,1)}, u32[]{:S(2)}) copy-start(bf16[128,1024]{1,0:T(8,128)(2,1)} %q.3) | copy-start | bytes 786436
  19.4 1.6 %collective-permute-start.1 = (bf16[128,1024]{1,0:T(8,128)(2,1)S(1)}, bf16[128,1024]{1,0:T(8,128)(2,1)S(1)}, u32[]{:S(2)}, u32[]{:S(2)}) collective-permute-start(bf16[128,1024]{1,0:T(8,128)(2,1)S(1)} %fusion.3), channel_id=1, source_target_pairs={{0,1},{1,0},{2,3},{3,2},{4,5},{5,4},{6,7},{7,6},{8,16},{9,17},{10,... | collective-permute-start | bytes 786440 | tf_op jit(solution)/shard_map/ppermute | solution.py:222
  21.1 2.0 %copy-start.15 = (bf16[128,1024]{1,0:T(8,128)(2,1)}, bf16[128,1024]{1,0:T(8,128)(2,1)S(1)}, u32[]{:S(2)}) copy-start(bf16[128,1024]{1,0:T(8,128)(2,1)S(1)} %collective-permute-done.1) | copy-start | bytes 786436
  23.0 12.8 %collective-permute-start.2 = (bf16[128,1024]{1,0:T(8,128)(2,1)}, bf16[128,1024]{1,0:T(8,128)(2,1)S(1)}, u32[]{:S(2)}, u32[]{:S(2)}) collective-permute-start(bf16[128,1024]{1,0:T(8,128)(2,1)} %fusion.5), channel_id=1, source_target_pairs={{0,8},{1,9},{2,10},{3,11},{4,12},{5,13},{6,14},{7,15},{8,0},{9,1},... | collective-permute-start | bytes 786440 | tf_op jit(solution)/shard_map/ppermute | solution.py:222
  30.4 5.4 %copy-start.14 = (bf16[128,1024]{1,0:T(8,128)(2,1)S(1)}, bf16[128,1024]{1,0:T(8,128)(2,1)}, u32[]{:S(2)}) copy-start(bf16[128,1024]{1,0:T(8,128)(2,1)} %copy-done.13) | copy-start | bytes 786436
  30.5 5.4 %copy-start.16 = (bf16[128,1024]{1,0:T(8,128)(2,1)S(1)}, bf16[128,1024]{1,0:T(8,128)(2,1)}, u32[]{:S(2)}) copy-start(bf16[128,1024]{1,0:T(8,128)(2,1)} %copy-done.15) | copy-start | bytes 786436
  35.8 1.0 %copy-start.11 = (bf16[128,1024]{1,0:T(8,128)(2,1)S(1)}, bf16[128,1024]{1,0:T(8,128)(2,1)}, u32[]{:S(2)}) copy-start(bf16[128,1024]{1,0:T(8,128)(2,1)} %copy-done.10) | copy-start | bytes 786436
  40.0 1.4 %collective-permute-start.3 = (f32[32,1024]{1,0:T(8,128)S(1)}, f32[32,1024]{1,0:T(8,128)S(1)}, u32[]{:S(2)}, u32[]{:S(2)}) collective-permute-start(f32[32,1024]{1,0:T(8,128)S(1)} %slice_select_fusion), channel_id=1, source_target_pairs={{0,1},{1,0},{2,3},{3,2},{4,5},{5,4},{6,7},{7,6},{8,9},{9,8},{10,11... | collective-permute-start | bytes 393224 | tf_op jit(solution)/shard_map/ppermute | solution.py:177
  41.5 5.3 %collective-permute-start.6 = (bf16[32,1024]{1,0:T(8,128)(2,1)S(1)}, bf16[32,1024]{1,0:T(8,128)(2,1)S(1)}, u32[]{:S(2)}, u32[]{:S(2)}) collective-permute-start(bf16[32,1024]{1,0:T(8,128)(2,1)S(1)} %add_convert_fusion.1), channel_id=1, source_target_pairs={{0,6},{1,7},{2,4},{3,5},{4,2},{5,3},{6,0},{7,1},{8,14},{9,15},{10,... | collective-permute-start | bytes 196616 | tf_op jit(solution)/shard_map/ppermute | solution.py:177
  44.0 4.3 %collective-permute-start.5 = (bf16[32,1024]{1,0:T(8,128)(2,1)S(1)}, bf16[32,1024]{1,0:T(8,128)(2,1)S(1)}, u32[]{:S(2)}, u32[]{:S(2)}) collective-permute-start(bf16[32,1024]{1,0:T(8,128)(2,1)S(1)} %add_convert_fusion.1), channel_id=1, source_target_pairs={{0,4},{1,5},{2,6},{3,7},{4,0},{5,1},{6,2},{7,3},{8,12},{9,13},{10,... | collective-permute-start | bytes 196616 | tf_op jit(solution)/shard_map/ppermute | solution.py:177
  44.5 4.3 %collective-permute-start.4 = (bf16[32,1024]{1,0:T(8,128)(2,1)S(1)}, bf16[32,1024]{1,0:T(8,128)(2,1)S(1)}, u32[]{:S(2)}, u32[]{:S(2)}) collective-permute-start(bf16[32,1024]{1,0:T(8,128)(2,1)S(1)} %add_convert_fusion.1), channel_id=1, source_target_pairs={{0,2},{1,3},{2,0},{3,1},{4,6},{5,7},{6,4},{7,5},{8,10},{9,11},{10,... | collective-permute-start | bytes 196616 | tf_op jit(solution)/shard_map/ppermute | solution.py:177
  48.8 8.4 %copy-start.9 = (bf16[64,1024]{1,0:T(8,128)(2,1)S(1)}, bf16[64,1024]{1,0:T(8,128)(2,1)}, u32[]{:S(2)}) copy-start(bf16[64,1024]{1,0:T(8,128)(2,1)} %w.3) | copy-start | bytes 393220
  48.8 6.8 %collective-permute-start.9 = (bf16[32,1024]{1,0:T(8,128)(2,1)S(1)}, bf16[32,1024]{1,0:T(8,128)(2,1)S(1)}, u32[]{:S(2)}, u32[]{:S(2)}) collective-permute-start(bf16[32,1024]{1,0:T(8,128)(2,1)S(1)} %add_convert_fusion), channel_id=1, source_target_pairs={{0,24},{8,16},{16,8},{24,0},{1,25},{9,17},{17,9},{25,1},{2,26},{10... | collective-permute-start | bytes 196616 | tf_op jit(solution)/shard_map/ppermute | solution.py:177
  51.4 5.7 %collective-permute-start.8 = (bf16[32,1024]{1,0:T(8,128)(2,1)S(1)}, bf16[32,1024]{1,0:T(8,128)(2,1)S(1)}, u32[]{:S(2)}, u32[]{:S(2)}) collective-permute-start(bf16[32,1024]{1,0:T(8,128)(2,1)S(1)} %add_convert_fusion), channel_id=1, source_target_pairs={{0,16},{8,24},{16,0},{24,8},{1,17},{9,25},{17,1},{25,9},{2,18},{10... | collective-permute-start | bytes 196616 | tf_op jit(solution)/shard_map/ppermute | solution.py:177
  51.4 5.7 %collective-permute-start.7 = (bf16[32,1024]{1,0:T(8,128)(2,1)S(1)}, bf16[32,1024]{1,0:T(8,128)(2,1)S(1)}, u32[]{:S(2)}, u32[]{:S(2)}) collective-permute-start(bf16[32,1024]{1,0:T(8,128)(2,1)S(1)} %add_convert_fusion), channel_id=1, source_target_pairs={{0,8},{8,0},{16,24},{24,16},{1,9},{9,1},{17,25},{25,17},{2,10},{10... | collective-permute-start | bytes 196616 | tf_op jit(solution)/shard_map/ppermute | solution.py:177
  57.1 2.6 %collective-permute-start.10 = (f32[32,1024]{1,0:T(8,128)S(1)}, f32[32,1024]{1,0:T(8,128)S(1)}, u32[]{:S(2)}, u32[]{:S(2)}) collective-permute-start(f32[32,1024]{1,0:T(8,128)S(1)} %add_add_fusion), channel_id=1, source_target_pairs={{0,1},{1,0},{2,3},{3,2},{4,5},{5,4},{6,7},{7,6},{8,9},{9,8},{10,11... | collective-permute-start | bytes 393224 | tf_op jit(solution)/shard_map/ppermute | solution.py:177
  (5 other events, 3.8 us)
